TPU v7x, 32 devices: a whole 2x2x4 slice. The times are simulated.
32 devices in a mesh: fs: 8 (over z, y), tp: 4 (over x, core).
Axes of the slice: x: 2, y: 2, z: 4, core: 2. Of those that a mesh axis runs over, the one named last changes fastest.
Arguments:
- tokens: bfloat16 [4096, 2048], P(('fs', 'tp')), may hold values from -6 to 6
- gate_proj: bfloat16 [2048, 512], P('fs', 'tp'), may hold values from -0.125 to 0.125
- signal_proj: bfloat16 [2048, 512], P('fs', 'tp'), may hold values from -1.5467961 to 1.5467961
- spatial: bfloat16 [4, 128, 128], replicated, may hold values from -0.5 to 0.5
- signal_gain: bfloat16 [512], P('tp'), may hold values from 0.099609375 to 1.8984375
- mixer_out: bfloat16 [512, 2048], P('tp', 'fs'), may hold values from -0.25 to 0.25
- mixer_gain: bfloat16 [2048], replicated, may hold values from 0.099609375 to 1.8984375
- ffn_gate: bfloat16 [2048, 5632], P('fs', 'tp'), may hold values from -0.125 to 0.125
- ffn_value: bfloat16 [2048, 5632], P('fs', 'tp'), may hold values from -0.125 to 0.125
- conv_taps: bfloat16 [3, 5632], P(None, 'tp'), may hold values from -3.5 to 3.5
- ffn_down: bfloat16 [5632, 2048], P('tp', 'fs'), may hold values from -0.078125 to 0.078125
- output_gain: bfloat16 [2048], replicated, may hold values from 0.099609375 to 1.8984375
Outputs:
- result: bfloat16 [4096, 2048], P(('fs', 'tp'))
All inputs are finite; a program needn't handle non-finite values.
Results may differ from a plain program's by a relative error of at most 0.01.
Values may be sent and summed in bfloat16 or wider, within the bound.
A program may use at most 64 MiB of HBM per device.

v0:
```python
import functools
import math

import jax
import jax.numpy as jnp
from jax import lax
from jax.experimental import pallas as pl
from jax.experimental.pallas import tpu as pltpu
from jax.sharding import PartitionSpec as P

MIX_WIDTH = 512
HEAD_SIZE = 128
BLOCK = 128
SEGMENT = 64
LANES = 128
GV_PIECES = 4
DN_PIECES = 2
EPSILON = 1e-05
RESIDUAL_SCALE = math.sqrt(2.0)
MESH = pl.DeviceIdType.MESH
F32 = jnp.float32
BF16 = jnp.bfloat16


def normalize(values):
    row_mean = jnp.mean(values, axis=-1, keepdims=True)
    centred = values - row_mean
    spread = jnp.mean(centred * centred, axis=-1, keepdims=True)
    return centred * lax.rsqrt(spread + EPSILON)


def kernel(
    nz, ny, nx,
    tok, gs, mo, gv, dn, spatial, sgain, mgain, taps, ogain,
    out,
    gsb, mob, gvb, dnb, xin, stat, pm, prc, abm, pxr, mid, hin, hid, pb, rb, ab, xr, zb, zr,
    loc_sem, zs, zrs, ys, yrs, ts, trs,
):
    R, D = tok.shape
    C = mo.shape[0]
    cw = mo.shape[1]
    W = dn.shape[1]
    f = lax.axis_index("fs")
    t = lax.axis_index("tp")
    z, y = f // ny, f % ny
    x, c = t // 2, t % 2
    q = z % 2
    seq = nx * 2 * R

    def zpeer(d):
        return (lax.rem(z + d, nz) * ny + y, t)

    def ypeer(d):
        return (z * ny + lax.rem(y + d, ny), t)

    def xpeer(d):
        return (f, lax.rem(x + d, nx) * 2 + c)

    cpeer = (f, x * 2 + 1 - c)
    ppeer = ((z + 1 - 2 * q) * ny + y, t)

    def zsrc(d):
        return lax.rem(z + nz - d, nz)

    def ysrc(d):
        return lax.rem(y + ny - d, ny)

    def xsrc(d):
        return lax.rem(x + nx - d, nx)

    pending = []

    def send(src, dst, ssem, rsem, to):
        copy = pltpu.make_async_remote_copy(
            src_ref=src, dst_ref=dst, send_sem=ssem, recv_sem=rsem, device_id=to, device_id_type=MESH
        )
        copy.start()
        pending.append(copy)

    def arrived(dst, ssem, rsem, to):
        pltpu.make_async_remote_copy(
            src_ref=dst, dst_ref=dst, send_sem=ssem, recv_sem=rsem, device_id=to, device_id_type=MESH
        ).wait_recv()

    barrier = pltpu.get_barrier_semaphore()
    peers = [zpeer(d) for d in range(1, nz)] + [ypeer(d) for d in range(1, ny)]
    peers += [xpeer(d) for d in range(1, nx)] + [cpeer]
    for p in peers:
        pl.semaphore_signal(barrier, inc=1, device_id=p, device_id_type=MESH)
    pl.semaphore_wait(barrier, len(peers))

    gv_rows = gv.shape[1] // GV_PIECES
    dn_rows = W // DN_PIECES
    DN = 2 + GV_PIECES
    EARLY = DN - 2

    def slot(a, zz, yy):
        if a == 0:
            return gsb.at[zz, yy]
        if a == 1:
            return mob.at[zz, yy]
        if a < DN:
            return gvb.at[zz, yy, pl.ds((a - 2) * gv_rows, gv_rows)]
        return dnb.at[zz, yy, pl.ds((a - DN) * dn_rows, dn_rows)]

    def local(a, zz):
        if a == 0:
            return gs
        if a == 1:
            return mo
        if a < DN:
            return gv.at[zz % 2, pl.ds((a - 2) * gv_rows, gv_rows)]
        return dn.at[zz % 2, pl.ds((a - DN) * dn_rows, dn_rows)]

    def issue(a):
        own = pltpu.make_async_copy(local(a, z), slot(a, z, y), loc_sem.at[a])
        own.start()
        for d in range(1, nz):
            to = zpeer(d)
            send(local(a, lax.rem(z + d, nz)), slot(a, z, y), zs.at[a, d], zrs.at[a, d], to)
        for e in range(1, ny):
            send(local(a, z), slot(a, z, y), ys.at[a, 0, e], yrs.at[a, 0, e], ypeer(e))
        own.wait()

    def relay(a):
        for d in range(1, nz):
            zz = zsrc(d)
            arrived(slot(a, zz, y), zs.at[a, d], zrs.at[a, d], zpeer(d))
            for e in range(1, ny):
                send(slot(a, zz, y), slot(a, zz, y), ys.at[a, d, e], yrs.at[a, d, e], ypeer(e))

    def complete(a, d):
        zz = zsrc(d)
        for e in range(1, ny):
            yy = ysrc(e)
            arrived(slot(a, zz, yy), ys.at[a, d, e], yrs.at[a, d, e], ypeer(e))

    scope = jax.named_scope

    tslot = [0]

    def tsem():
        k = tslot[0]
        tslot[0] += 1
        return ts.at[k], trs.at[k]

    issue(0)
    issue(1)

    xin[x, c] = normalize(tok[...].astype(F32)).astype(BF16)
    s1 = [tsem() for _ in range(nx)]
    s2 = [tsem() for _ in range(nx)]
    for d in range(1, nx):
        send(xin.at[x, c], xin.at[x, c], *s1[d], xpeer(d))
    send(xin.at[x, c], xin.at[x, c], *s2[0], cpeer)
    with scope("relay_mix"):
        relay(0)
        relay(1)
    for a in range(2, EARLY):
        issue(a)
    for d in range(1, nx):
        arrived(xin.at[xsrc(d), c], *s1[d], xpeer(d))
        send(xin.at[xsrc(d), c], xin.at[xsrc(d), c], *s2[d], cpeer)
    for d in range(nx):
        arrived(xin.at[xsrc(d), 1 - c], *s2[d], cpeer)
    with scope("complete_gs"):
        for d in range(nz):
            complete(0, d)

    kdim = gs.shape[0]
    pre = jnp.dot(
        xin[...].reshape(seq, D), gsb[...].reshape(nz * ny * kdim, 2 * C), preferred_element_type=F32
    )
    branch_gate = jax.nn.gelu(pre[:, :C])
    branch_signal = jax.nn.gelu(pre[:, C:])
    total = jnp.sum(branch_signal, axis=1, keepdims=True)
    square = jnp.sum(branch_signal * branch_signal, axis=1, keepdims=True)
    lane = lax.broadcasted_iota(jnp.int32, (seq, LANES), 1)
    stat[0] = jnp.where(lane == 0, total, square).T[:8]
    sc = tsem()
    send(stat.at[0], stat.at[1], *sc, cpeer)
    arrived(stat.at[1], *sc, cpeer)
    stat[2] = stat[0] + stat[1]
    sx = [tsem() for _ in range(nx)]
    for d in range(1, nx):
        send(stat.at[2], stat.at[2 + d], *sx[d], xpeer(d))
    for d in range(1, nx):
        arrived(stat.at[2 + d], *sx[d], xpeer(d))
    summed = stat[2]
    for d in range(1, nx):
        summed = summed + stat[2 + d]
    back = summed.T
    row_mean = back[:, 0:1] / MIX_WIDTH
    spread = back[:, 1:2] / MIX_WIDTH - row_mean * row_mean
    spatial_input = (
        (branch_signal - row_mean) * lax.rsqrt(spread + EPSILON) * sgain[...].astype(F32)
    ).astype(BF16)
    rows_i = lax.broadcasted_iota(jnp.int32, (BLOCK, BLOCK), 0) // SEGMENT
    cols_i = lax.broadcasted_iota(jnp.int32, (BLOCK, BLOCK), 1) // SEGMENT
    own = spatial[t * C // HEAD_SIZE]
    own = jnp.where(cols_i <= rows_i, own, jnp.zeros_like(own))
    with scope("complete_mo"):
        for d in range(nz):
            complete(1, d)
    gated = jnp.concatenate(
        [
            branch_gate[b * BLOCK:(b + 1) * BLOCK]
            * jnp.dot(own, spatial_input[b * BLOCK:(b + 1) * BLOCK], preferred_element_type=F32)
            for b in range(seq // BLOCK)
        ],
        axis=0,
    ).astype(BF16)
    for k in range(nz * ny):
        part = jnp.dot(gated, mob[k // ny, k % ny], preferred_element_type=F32).astype(BF16)
        for b in range(nx * 2):
            pm[b % 2, b // 2, :, k * cw:(k + 1) * cw] = part[b * R:(b + 1) * R]
    sc = tsem()
    send(pm.at[1 - c], prc, *sc, cpeer)
    arrived(prc, *sc, cpeer)
    for b in range(nx):
        abm[b] = (pm[c, b].astype(F32) + prc[b].astype(F32)).astype(BF16)
    sx = [tsem() for _ in range(nx)]
    for d in range(1, nx):
        send(abm.at[lax.rem(x + d, nx)], pxr.at[d - 1], *sx[d], xpeer(d))
    with scope("mix_x"):
        for d in range(1, nx):
            arrived(pxr.at[d - 1], *sx[d], xpeer(d))
    mix_out = pm[c, x].astype(F32) + prc[x].astype(F32)
    for d in range(1, nx):
        mix_out = mix_out + pxr[d - 1].astype(F32)
    mid[...] = (
        normalize(RESIDUAL_SCALE * tok[...].astype(F32) + mix_out) * mgain[...].astype(F32)
    ).astype(BF16)
    hin[q, x, c] = normalize(mid[...].astype(F32)).astype(BF16)

    sp = tsem()
    send(hin.at[q, x, c], hin.at[q, x, c], *sp, ppeer)
    sx = [[tsem() for _ in range(nx)] for _ in range(2)]
    sy = [[tsem() for _ in range(nx)] for _ in range(2)]
    for d in range(1, nx):
        send(hin.at[q, x, c], hin.at[q, x, c], *sx[0][d], xpeer(d))
    send(hin.at[q, x, c], hin.at[q, x, c], *sy[0][0], cpeer)
    for a in range(EARLY, DN + DN_PIECES):
        issue(a)
    for a in range(2, DN - 1):
        with scope(f"relay_gv{a - 2}"):
            relay(a)
    with scope("relay_gv3"):
        relay(DN - 1)
    with scope("pair_rows"):
        arrived(hin.at[1 - q, x, c], *sp, ppeer)
    for d in range(1, nx):
        send(hin.at[1 - q, x, c], hin.at[1 - q, x, c], *sx[1][d], xpeer(d))
    send(hin.at[1 - q, x, c], hin.at[1 - q, x, c], *sy[1][0], cpeer)
    with scope("rows_x"):
        for k, s in enumerate((q, 1 - q)):
            for d in range(1, nx):
                arrived(hin.at[s, xsrc(d), c], *sx[k][d], xpeer(d))
                send(hin.at[s, xsrc(d), c], hin.at[s, xsrc(d), c], *sy[k][d], cpeer)
    with scope("rows_core"):
        for k, s in enumerate((q, 1 - q)):
            for d in range(nx):
                arrived(hin.at[s, xsrc(d), 1 - c], *sy[k][d], cpeer)
    with scope("relay_dn0"):
        relay(DN)
    with scope("complete_gv"):
        for a in range(2, DN):
            for d in range(nz):
                complete(a, d)

    for s in range(2):

        def column(j, carry):
            at = pl.multiple_of(j * LANES, LANES)
            at_v = pl.multiple_of(W + j * LANES, LANES)
            lhs = hin[s].reshape(seq, D)
            wg = gvb[:, :, :, pl.ds(at, LANES)].reshape(D, LANES)
            wv = gvb[:, :, :, pl.ds(at_v, LANES)].reshape(D, LANES)
            both = jnp.dot(lhs, jnp.concatenate([wg, wv], axis=1), preferred_element_type=F32)
            gate = both[:, :LANES]
            value = both[:, LANES:]
            tap = taps[q, :, pl.ds(at, LANES)].astype(F32)
            row = lax.broadcasted_iota(jnp.int32, gate.shape, 0)
            one = jnp.where(row >= 1, pltpu.roll(gate, 1, 0), 0.0)
            two = jnp.where(row >= 2, pltpu.roll(gate, 2, 0), 0.0)
            conv = tap[0:1] * two + tap[1:2] * one + tap[2:3] * gate
            hid[s, :, pl.ds(at, LANES)] = (jax.nn.silu(conv) * value).astype(BF16)
            return carry

        with scope("gate_value"):
            lax.fori_loop(0, W // LANES, column, 0)
        if s == 0:
            with scope("relay_dn1"):
                for a in range(DN + 1, DN + DN_PIECES):
                    relay(a)

    sc = [[tsem() for _ in range(2)] for _ in range(nz)]
    sx = [[[tsem() for _ in range(nx)] for _ in range(2)] for _ in range(nz)]
    zbase = tslot[0]
    tslot[0] += nz
    turns = (1 - q, q)

    def down(i):
        g = zsrc(i)
        for k, s in enumerate(turns):
            for yy in range(ny):
                part = jnp.dot(hid[s], dnb[g, yy], preferred_element_type=F32).astype(BF16)
                for b in range(nx * 2):
                    pb[b % 2, g, s, b // 2, :, yy * cw:(yy + 1) * cw] = part[b * R:(b + 1) * R]
            send(pb.at[1 - c, g, s], rb.at[i, s], *sc[i][k], cpeer)

    def over_x(i):
        g = zsrc(i)
        for k, s in enumerate(turns):
            arrived(rb.at[i, s], *sc[i][k], cpeer)
            for b in range(nx):
                ab[i, s, b] = (pb[c, g, s, b].astype(F32) + rb[i, s, b].astype(F32)).astype(BF16)
            for d in range(1, nx):
                send(ab.at[i, s, lax.rem(x + d, nx)], xr.at[i, d - 1, s], *sx[i][k][d], xpeer(d))

    def over_z(i):
        g = zsrc(i)
        for k, s in enumerate(turns):
            for d in range(1, nx):
                arrived(xr.at[i, d - 1, s], *sx[i][k][d], xpeer(d))
            acc = ab[i, s, x].astype(F32)
            for d in range(1, nx):
                acc = acc + xr[i, d - 1, s].astype(F32)
            zb[g, s] = acc.astype(BF16)
            if k == 0:
                send(zb.at[g, s], zr.at[g], ts.at[zbase + g], trs.at[zbase + g], ppeer)

    for i in range(nz):
        with scope(f"complete_dn{i}"):
            for a in range(DN, DN + DN_PIECES):
                complete(a, i)
        with scope(f"down{i}"):
            down(i)
        if i >= 1:
            over_x(i - 1)
        if i >= 2:
            over_z(i - 2)
    with scope("tail_x"):
        over_x(nz - 1)
        over_z(nz - 2)
        over_z(nz - 1)
    with scope("tail_z"):
        for g in range(nz):
            arrived(zr.at[g], ts.at[zbase + g], trs.at[zbase + g], ppeer)
    ffn_out = jnp.concatenate(
        [zb[g, q].astype(F32) + zr[g].astype(F32) for g in range(nz)], axis=1
    )
    out[...] = (
        normalize(RESIDUAL_SCALE * mid[...].astype(F32) + ffn_out) * ogain[...].astype(F32)
    ).astype(BF16)
    for copy in pending:
        copy.wait_send()


def shards(nf, nt, ny, tokens, gate_proj, signal_proj, spatial, signal_gain, mixer_out, mixer_gain, ffn_gate, ffn_value, conv_taps, ffn_down, output_gain):
    nz = nf // ny
    nx = nt // 2
    R, D = tokens.shape
    C = gate_proj.shape[1]
    H = ffn_gate.shape[1]
    W = -(-H // (2 * LANES)) * LANES
    cw = mixer_out.shape[1]
    seq = nx * 2 * R

    gs = jnp.concatenate([gate_proj, signal_proj], axis=1)
    gv = jnp.stack(
        [
            jnp.concatenate([ffn_gate[:, :W], ffn_value[:, :W]], axis=1),
            jnp.concatenate([ffn_gate[:, H - W:], ffn_value[:, H - W:]], axis=1),
        ]
    )
    fresh = (jnp.arange(W) >= 2 * W - H)[:, None]
    low = ffn_down[H - W:]
    dn = jnp.stack([ffn_down[:W], jnp.where(fresh, low, jnp.zeros_like(low))])
    taps = jnp.stack([conv_taps[:, :W], conv_taps[:, H - W:]])
    gw = ny * cw
    vm = pltpu.VMEM
    n_w = 2 + GV_PIECES + DN_PIECES
    dma = pltpu.SemaphoreType.DMA
    n_t = 2 * nx + 1 + nx + 1 + nx + 1 + 4 * nx + nz * (3 + 2 * nx)
    scratch = [
        vm((nz, ny) + gs.shape, BF16),
        vm((nz, ny) + mixer_out.shape, BF16),
        vm((nz, ny) + gv.shape[1:], BF16),
        vm((nz, ny) + dn.shape[1:], BF16),
        vm((nx, 2, R, D), BF16),
        vm((2 + nx, 8, seq), F32),
        vm((2, nx, R, D), BF16),
        vm((nx, R, D), BF16),
        vm((nx, R, D), BF16),
        vm((nx - 1, R, D), BF16),
        vm((R, D), BF16),
        vm((2, nx, 2, R, D), BF16),
        vm((2, seq, W), BF16),
        vm((2, nz, 2, nx, R, gw), BF16),
        vm((nz, 2, nx, R, gw), BF16),
        vm((nz, 2, nx, R, gw), BF16),
        vm((nz, nx - 1, 2, R, gw), BF16),
        vm((nz, 2, R, gw), BF16),
        vm((nz, R, gw), BF16),
        dma((n_w,)),
        dma((n_w, nz)),
        dma((n_w, nz)),
        dma((n_w, nz, ny)),
        dma((n_w, nz, ny)),
        dma((n_t,)),
        dma((n_t,)),
    ]
    return pl.pallas_call(
        functools.partial(kernel, nz, ny, nx),
        out_shape=jax.ShapeDtypeStruct((R, D), BF16),
        in_specs=[pl.BlockSpec(memory_space=pltpu.VMEM)] * 10,
        out_specs=pl.BlockSpec(memory_space=pltpu.VMEM),
        scratch_shapes=scratch,
        compiler_params=pltpu.CompilerParams(
            collective_id=0, has_side_effects=True, vmem_limit_bytes=67043328
        ),
    )(
        tokens, gs, mixer_out, gv, dn, spatial, signal_gain[None], mixer_gain[None], taps, output_gain[None]
    )


def solution(mesh):
    nf, nt = mesh.shape["fs"], mesh.shape["tp"]
    ny = 2 ** (int(math.log2(nf // 2)) // 2)
    in_specs = (
        P(("fs", "tp"), None),
        P("fs", "tp"),
        P("fs", "tp"),
        P(),
        P("tp"),
        P("tp", "fs"),
        P(),
        P("fs", "tp"),
        P("fs", "tp"),
        P(None, "tp"),
        P("tp", "fs"),
        P(),
    )
    return jax.shard_map(
        functools.partial(shards, nf, nt, ny),
        mesh=mesh,
        in_specs=in_specs,
        out_specs=P(("fs", "tp"), None),
        check_vma=False,
    )
```

profile of v0, /device:TPU:0, one launch (start us, length us, event | category | flops | bytes accessed | tf_op | source)
XLA Modules:
  0.0 177.0 jit_solution(4960967900465220113)
XLA Ops:
  0.0 1.2 fusion.1
  1.2 0.1 copy-done
  1.3 0.1 fusion
  1.4 0.1 maximum_bitcast_fusion
  1.5 0.0 copy-start.1
  1.5 1.3 pad_maximum_fusion.gv
  2.8 0.0 copy-done.1
  2.8 0.0 copy-start.2
  2.9 0.0 copy-start.3
  2.9 0.0 copy-start.5
  2.9 0.0 copy-start.6
  2.9 0.2 slice_bitcast_fusion
  3.1 0.9 pad_maximum_fusion.1.dn
  4.0 0.0 copy-done.4
  4.0 0.6 pad_maximum_fusion.3.taps
  4.6 0.0 copy-done.2
  4.6 0.0 copy-done.3
  4.6 0.7 pad_maximum_fusion.2.gs
  5.3 0.0 copy-done.5
  5.3 0.6 broadcast_in_dim.24.mgain
  5.9 0.0 copy-done.6
  5.9 0.6 broadcast_in_dim.25.ogain
  6.5 168.6 %shard_map.118 = bf16[128,2048]{1,0:T(8,128)(2,1)} custom-call(bf16[128,2048]{1,0:T(8,128)(2,1)} %tok.1, bf16[256,256]{1,0:T(8,128)(2,1)} %pad_maximum_fusion.2.gs, bf16[128,256]{1,0:T(8,128)(2,1)} %mo.1, bf16[2,256,1536]{2,1,0:T(8,128)(2,1)} %pad_maximum_fusion.gv, bf16[2,768,256]{2,1,0:T(8,128)(2,1)} %pad_maximum_fusion.1.dn, ...), custom_call_target="tpu_custom_call" | custom-call | tf_op jit(solution)/shard_map/pallas_call | solution.py:414
  175.1 1.9 %copy.14 = bf16[128,2048]{1,0:T(8,128)(2,1)} copy(bf16[128,2048]{1,0:T(8,128)(2,1)} %shard_map.118) | data formatting | bytes 1048576
  (4 shorter events, 0.0 us)
Async XLA Ops:
  0.0 1.3 copy-start
  1.5 1.3 copy-start.1
  2.8 1.2 copy-start.4
  2.8 1.8 %copy-start.2 = (bf16[256,128]{1,0:T(8,128)(2,1)S(1)}, bf16[256,128]{1,0:T(8,128)(2,1)}, u32[]{:S(2)}) copy-start(bf16[256,128]{1,0:T(8,128)(2,1)} %param.14) | copy-start | bytes 196612
  2.9 1.8 %copy-start.3 = (bf16[256,128]{1,0:T(8,128)(2,1)S(1)}, bf16[256,128]{1,0:T(8,128)(2,1)}, u32[]{:S(2)}) copy-start(bf16[256,128]{1,0:T(8,128)(2,1)} %param.13) | copy-start | bytes 196612
  2.9 2.4 %copy-start.5 = (bf16[2048]{0:T(1024)(128)(2,1)S(1)}, bf16[2048]{0:T(1024)(128)(2,1)}, u32[]{:S(2)}) copy-start(bf16[2048]{0:T(1024)(128)(2,1)} %param.18) | copy-start | bytes 12292
  2.9 3.0 %copy-start.6 = (bf16[2048]{0:T(1024)(128)(2,1)S(1)}, bf16[2048]{0:T(1024)(128)(2,1)}, u32[]{:S(2)}) copy-start(bf16[2048]{0:T(1024)(128)(2,1)} %param.23) | copy-start | bytes 12292
where the time goes:
time: 178 us; the launch traced here: 177 us
  Pallas kernels  169 us (95%)
  local copies, waits for them, and re-layouts  4.51 us (3%)
  other arithmetic  3.8 us (2%)
    pallas_call x1, Pallas kernels, shards(): pl.pallas_call(functools.partial(kernel, nz, ny, nx), out_shape=jax.Shape...  169 us

commit v1 on v0

v1 whole, which is shorter than its diff:
```python
import functools
import math

import jax
import jax.numpy as jnp
from jax import lax
from jax.experimental import pallas as pl
from jax.experimental.pallas import tpu as pltpu
from jax.sharding import PartitionSpec as P

MIX_WIDTH = 512
HEAD_SIZE = 128
BLOCK = 128
SEGMENT = 64
LANES = 128
GV_PIECES = 4
DN_PIECES = 2
EARLY = 2
EPSILON = 1e-05
RESIDUAL_SCALE = math.sqrt(2.0)
MESH = pl.DeviceIdType.MESH
F32 = jnp.float32
BF16 = jnp.bfloat16


def normalize(values):
    row_mean = jnp.mean(values, axis=-1, keepdims=True)
    centred = values - row_mean
    spread = jnp.mean(centred * centred, axis=-1, keepdims=True)
    return centred * lax.rsqrt(spread + EPSILON)


def kernel(
    nz, ny, nx, full, rem, subs, packed,
    tok, gp, sp_, mo, fg, fv, gt, vt, dn, spatial, sgain, mgain, taps, ogain,
    out,
    gsb, mob, gvb, dnb, tails, mixed, xin, stat, pm, prc, abm, pxr, mid, hin, hid, pb, rb, ab, xr, zb, zr,
    loc_sem, gzs, gzr, gys, gyr, mzs, mzr, mys, myr, zs, zrs, ys, yrs, ts, trs,
):
    R, D = tok.shape
    C, cw = mo.shape
    K = fg.shape[0]
    F = full
    W = full + rem
    MW = mixed.shape[2]
    f = lax.axis_index("fs")
    t = lax.axis_index("tp")
    z, y = f // ny, f % ny
    x, c = t // 2, t % 2
    q = z % 2
    seq = nx * 2 * R
    gw = ny * cw

    def zsrc(d):
        zz = z
        for bit in (1 << k for k in range(d.bit_length())):
            if d & bit:
                zz = zz + bit - 2 * bit * ((z // bit) % 2)
        return zz

    def zpeer(d):
        return (zsrc(d) * ny + y, t)

    def ypeer(e):
        return (z * ny + lax.rem(y + e, ny), t)

    def xpeer(d):
        return (f, lax.rem(x + d, nx) * 2 + c)

    def tpeer(d, e):
        return (f, lax.rem(x + d, nx) * 2 + (c if e == 0 else 1 - c))

    cpeer = (f, x * 2 + 1 - c)
    ppeer = ((z + 1 - 2 * q) * ny + y, t)

    def ysrc(e):
        return lax.rem(y + ny - e, ny)

    def xsrc(d):
        return lax.rem(x + nx - d, nx)

    pending = []

    def remote(src, dst, ssem, rsem, to):
        return pltpu.make_async_remote_copy(
            src_ref=src, dst_ref=dst, send_sem=ssem, recv_sem=rsem, device_id=to, device_id_type=MESH
        )

    def when(cond, action):
        if cond is None:
            action()
        else:
            pl.when(cond)(action)

    def send(src, dst, ssem, rsem, to, cond=None):
        copy = remote(src, dst, ssem, rsem, to)
        when(cond, lambda: copy.start())
        pending.append((copy, cond))

    def arrived(dst, ssem, rsem, to):
        remote(dst, dst, ssem, rsem, to).wait_recv()

    scope = jax.named_scope
    tslot = [0]

    def tsem():
        k = tslot[0]
        tslot[0] += 1
        return ts.at[k], trs.at[k]

    gv_rows = K // GV_PIECES
    dn_rows = W // DN_PIECES
    DN = GV_PIECES

    def parts(a, h, zz, yy):
        if a < DN:
            rows = pl.ds(a * gv_rows, gv_rows)
            dst = gvb.at[zz, yy]
            at = pl.multiple_of(h * F, LANES)
            return [
                (fg.at[rows, pl.ds(at, F)], dst.at[rows, pl.ds(0, F)]),
                (fv.at[rows, pl.ds(at, F)], dst.at[rows, pl.ds(F, F)]),
                (mixed.at[h, rows], dst.at[rows, pl.ds(2 * F, MW)]),
            ]
        lo, hi = (a - DN) * dn_rows, (a - DN + 1) * dn_rows
        dst = dnb.at[zz, yy]
        found = []
        if lo < F:
            n = min(hi, F) - lo
            found.append((dn.at[pl.ds(pl.multiple_of(h * F + lo, 16), n)], dst.at[pl.ds(lo, n)]))
        if hi > F:
            s = max(lo, F)
            n = hi - s
            found.append(
                (dn.at[pl.ds(pl.multiple_of(2 * F + h * rem + s - F, 16), n)], dst.at[pl.ds(s, n)])
            )
        return found

    def slot(a, zz, yy):
        if a < DN:
            return gvb.at[zz, yy, pl.ds(a * gv_rows, gv_rows)]
        return dnb.at[zz, yy, pl.ds((a - DN) * dn_rows, dn_rows)]

    lk = [0]
    held = {}

    def fetch(key, src, dst):
        copy = pltpu.make_async_copy(src, dst, loc_sem.at[lk[0]])
        lk[0] += 1
        copy.start()
        held.setdefault(key, []).append(copy)

    def ready(key):
        for copy in held.pop(key):
            copy.wait()

    if packed:
        fetch("gs", gp, gsb.at[z, y])
    else:
        fetch("gs", gp, gsb.at[z, y, :, pl.ds(0, C)])
        fetch("gs", sp_, gsb.at[z, y, :, pl.ds(C, C)])
    fetch("mo", mo, mob.at[z, y])
    T = tails.shape[2]
    if packed:
        fetch("tails", gt, tails.at[0])
        fetch("tails", vt, tails.at[1])
    else:
        fetch("tails", gt.at[:, pl.ds(2 * F, T)], tails.at[0])
        fetch("tails", vt.at[:, pl.ds(2 * F, T)], tails.at[1])
    for a in range(DN):
        for src, dst in parts(a, q, z, y)[:2]:
            fetch("gv", src, dst)
    for a in range(DN, DN + DN_PIECES):
        for src, dst in parts(a, q, z, y):
            fetch("dn", src, dst)

    barrier = pltpu.get_barrier_semaphore()
    peers = [zpeer(d) for d in range(1, nz)] + [ypeer(e) for e in range(1, ny)]
    peers += [tpeer(d, e) for d in range(nx) for e in range(2) if d + e]
    for p in peers:
        pl.semaphore_signal(barrier, inc=1, device_id=p, device_id_type=MESH)

    ready("tails")
    for h in range(2):
        for k in range(2):
            mixed[h, :, k * (MW // 2):k * (MW // 2) + rem] = tails[k, :, h * rem:(h + 1) * rem]
    for k in range(2):
        part = tails[k].astype(F32)
        part = jnp.where(q == 0, part[:, :rem], part[:, rem:2 * rem]).astype(BF16)
        gvb[z, y, :, 2 * F + k * (MW // 2):2 * F + k * (MW // 2) + rem] = part
    ready("gs")
    ready("mo")
    pl.semaphore_wait(barrier, len(peers))

    def issue_z(a, d):
        for src, dst in parts(a, zsrc(d) % 2, z, y):
            remote(src, dst, zs.at[a, d], zrs.at[a, d], zpeer(d)).start()
        whole = slot(a, z, y)
        pending.append((remote(whole, whole, zs.at[a, d], zrs.at[a, d], zpeer(d)), None))

    def issue_all(a):
        for d in range(1, nz):
            issue_z(a, d)

    def issue_y(a):
        for e in range(1, ny):
            send(slot(a, z, y), slot(a, z, y), ys.at[a, 0, e], yrs.at[a, 0, e], ypeer(e))

    def relay(a, d):
        zz = zsrc(d)
        arrived(slot(a, zz, y), zs.at[a, d], zrs.at[a, d], zpeer(d))
        for e in range(1, ny):
            send(slot(a, zz, y), slot(a, zz, y), ys.at[a, d, e], yrs.at[a, d, e], ypeer(e))

    def complete(a, d, e):
        zz, yy = zsrc(d), ysrc(e)
        arrived(slot(a, zz, yy), ys.at[a, d, e], yrs.at[a, d, e], ypeer(e))

    own_gs, own_mo = gsb.at[z, y], mob.at[z, y]
    for d in range(1, nz):
        send(own_gs, own_gs, gzs.at[d], gzr.at[d], zpeer(d))
    for d in range(1, nz):
        send(own_mo, own_mo, mzs.at[d], mzr.at[d], zpeer(d))
    for e in range(1, ny):
        send(own_gs, own_gs, gys.at[0, e], gyr.at[0, e], ypeer(e))
    for e in range(1, ny):
        send(own_mo, own_mo, mys.at[0, e], myr.at[0, e], ypeer(e))
    ready("gv")
    issue_y(0)

    xin[x, c] = normalize(tok[...].astype(F32)).astype(BF16)
    s1 = [tsem() for _ in range(nx)]
    s2 = [tsem() for _ in range(nx)]
    for d in range(1, nx):
        send(xin.at[x, c], xin.at[x, c], *s1[d], xpeer(d))
    send(xin.at[x, c], xin.at[x, c], *s2[0], cpeer)

    def pass_on(buf, d, zsem, zrsem, ysem, yrsem):
        block = buf.at[zsrc(d), y]
        arrived(block, zsem.at[d], zrsem.at[d], zpeer(d))
        for e in range(1, ny):
            send(block, block, ysem.at[d, e], yrsem.at[d, e], ypeer(e))

    for d in range(1, nz):
        with scope(f"relay_gs{d}"):
            pass_on(gsb, d, gzs, gzr, gys, gyr)
    for d in range(1, nz):
        with scope(f"relay_mo{d}"):
            pass_on(mob, d, mzs, mzr, mys, myr)
    issue_all(0)
    issue_all(1)
    ready("dn")
    for a in range(1, DN + DN_PIECES):
        issue_y(a)
    with scope("xin"):
        for d in range(1, nx):
            arrived(xin.at[xsrc(d), c], *s1[d], xpeer(d))
            send(xin.at[xsrc(d), c], xin.at[xsrc(d), c], *s2[d], cpeer)
        for d in range(nx):
            arrived(xin.at[xsrc(d), 1 - c], *s2[d], cpeer)
    with scope("complete_gs"):
        for d in range(nz):
            for e in range(1, ny):
                yy = ysrc(e)
                arrived(gsb.at[zsrc(d), yy], gys.at[d, e], gyr.at[d, e], ypeer(e))

    with scope("mix_in"):
        pre = jnp.dot(xin[...].reshape(seq, D), gsb[...].reshape(D, 2 * C), preferred_element_type=F32)
        branch_signal = jax.nn.gelu(pre[:, C:])
        total = jnp.sum(branch_signal, axis=1, keepdims=True)
        square = jnp.sum(branch_signal * branch_signal, axis=1, keepdims=True)
        lane = lax.broadcasted_iota(jnp.int32, (seq, LANES), 1)
        stat[0] = jnp.where(lane == 0, total, square).T[:8]
    others = [(d, e) for d in range(nx) for e in range(2) if d + e]
    sx = {}
    for d, e in others:
        sx[d, e] = tsem()
        send(stat.at[0], stat.at[2 * d + e], *sx[d, e], tpeer(d, e))
    branch_gate = jax.nn.gelu(pre[:, :C])
    with scope("stats"):
        summed = stat[0]
        for d, e in others:
            arrived(stat.at[2 * d + e], *sx[d, e], tpeer(d, e))
            summed = summed + stat[2 * d + e]
    with scope("complete_mo"):
        for d in range(nz):
            for e in range(1, ny):
                arrived(mob.at[zsrc(d), ysrc(e)], mys.at[d, e], myr.at[d, e], ypeer(e))
    with scope("mix_out"):
        back = summed.T
        row_mean = back[:, 0:1] / MIX_WIDTH
        spread = back[:, 1:2] / MIX_WIDTH - row_mean * row_mean
        spatial_input = (
            (branch_signal - row_mean) * lax.rsqrt(spread + EPSILON) * sgain[...].astype(F32)
        ).astype(BF16)
        rows_i = lax.broadcasted_iota(jnp.int32, (BLOCK, BLOCK), 0) // SEGMENT
        cols_i = lax.broadcasted_iota(jnp.int32, (BLOCK, BLOCK), 1) // SEGMENT
        own = spatial[t * C // HEAD_SIZE]
        own = jnp.where(cols_i <= rows_i, own, jnp.zeros_like(own))
        gated = jnp.concatenate(
            [
                branch_gate[b * BLOCK:(b + 1) * BLOCK]
                * jnp.dot(own, spatial_input[b * BLOCK:(b + 1) * BLOCK], preferred_element_type=F32)
                for b in range(seq // BLOCK)
            ],
            axis=0,
        ).astype(BF16)
        for k in range(nz * ny):
            part = jnp.dot(gated, mob[k // ny, k % ny], preferred_element_type=F32).astype(BF16)
            for b in range(nx * 2):
                pm[b % 2, b // 2, :, k * cw:(k + 1) * cw] = part[b * R:(b + 1) * R]
    sc = tsem()
    send(pm.at[1 - c], prc, *sc, cpeer)
    with scope("mix_core"):
        arrived(prc, *sc, cpeer)
    for b in range(nx):
        abm[b] = (pm[c, b].astype(F32) + prc[b].astype(F32)).astype(BF16)
    sx = [tsem() for _ in range(nx)]
    for d in range(1, nx):
        send(abm.at[lax.rem(x + d, nx)], pxr.at[d - 1], *sx[d], xpeer(d))
    with scope("relay_gv0"):
        for d in range(1, nz):
            relay(0, d)
    issue_all(2)
    with scope("mix_x"):
        for d in range(1, nx):
            arrived(pxr.at[d - 1], *sx[d], xpeer(d))
    with scope("mid"):
        mix_out = pm[c, x].astype(F32) + prc[x].astype(F32)
        for d in range(1, nx):
            mix_out = mix_out + pxr[d - 1].astype(F32)
        mid[...] = (
            normalize(RESIDUAL_SCALE * tok[...].astype(F32) + mix_out) * mgain[...].astype(F32)
        ).astype(BF16)
        hin[q, x, c] = normalize(mid[...].astype(F32)).astype(BF16)

    sp = tsem()
    send(hin.at[q, x, c], hin.at[q, x, c], *sp, ppeer)
    sx = [[tsem() for _ in range(nx)] for _ in range(2)]
    sy = [[tsem() for _ in range(nx)] for _ in range(2)]
    for d in range(1, nx):
        send(hin.at[q, x, c], hin.at[q, x, c], *sx[0][d], xpeer(d))
    send(hin.at[q, x, c], hin.at[q, x, c], *sy[0][0], cpeer)
    with scope("relay_gv1"):
        for d in range(1, nz):
            relay(1, d)

    def rows_over(k, s):
        for d in range(1, nx):
            arrived(hin.at[s, xsrc(d), c], *sx[k][d], xpeer(d))
            send(hin.at[s, xsrc(d), c], hin.at[s, xsrc(d), c], *sy[k][d], cpeer)

    with scope("rows_x0"):
        rows_over(0, q)
    for a in range(2, DN):
        with scope(f"relay_gv{a}"):
            for d in range(1, nz):
                relay(a, d)
                if d == 1:
                    issue_all(a + 1)
                elif d == nz - 1 and a == DN - 1:
                    issue_all(a + 2)
        if a == 2:
            with scope("pair_rows"):
                arrived(hin.at[1 - q, x, c], *sp, ppeer)
            for d in range(1, nx):
                send(hin.at[1 - q, x, c], hin.at[1 - q, x, c], *sx[1][d], xpeer(d))
            send(hin.at[1 - q, x, c], hin.at[1 - q, x, c], *sy[1][0], cpeer)
    with scope("rows_x1"):
        rows_over(1, 1 - q)
    with scope("rows_core"):
        for k, s in enumerate((q, 1 - q)):
            for d in range(nx):
                arrived(hin.at[s, xsrc(d), 1 - c], *sy[k][d], cpeer)
    with scope("complete_gv"):
        for a in range(DN):
            for d in range(nz):
                for e in range(1, ny):
                    complete(a, d, e)

    def gate_value(s):
        def finish(gate, value, tap):
            row = lax.broadcasted_iota(jnp.int32, gate.shape, 0)
            one = jnp.where(row >= 1, pltpu.roll(gate, 1, 0), 0.0)
            two = jnp.where(row >= 2, pltpu.roll(gate, 2, 0), 0.0)
            conv = tap[0:1] * two + tap[1:2] * one + tap[2:3] * gate
            return (jax.nn.silu(conv) * value).astype(BF16)

        def column(j, carry):
            at = pl.multiple_of(j * LANES, LANES)
            at_v = pl.multiple_of(F + j * LANES, LANES)
            lhs = hin[s].reshape(seq, D)
            wg = gvb[:, :, :, pl.ds(at, LANES)].reshape(D, LANES)
            wv = gvb[:, :, :, pl.ds(at_v, LANES)].reshape(D, LANES)
            both = jnp.dot(lhs, jnp.concatenate([wg, wv], axis=1), preferred_element_type=F32)
            tap = taps[:, pl.ds(pl.multiple_of(q * F + j * LANES, LANES), LANES)].astype(F32)
            hid[s, :, pl.ds(at, LANES)] = finish(both[:, :LANES], both[:, LANES:], tap)
            return carry

        lax.fori_loop(0, F // LANES, column, 0)
        lhs = hin[s].reshape(seq, D)
        both = jnp.dot(lhs, gvb[:, :, :, 2 * F:].reshape(D, MW), preferred_element_type=F32)
        tail = taps[:, 2 * F:2 * F + 2 * rem].astype(F32)
        tail = jnp.where(q == 0, tail[:, :rem], tail[:, rem:])
        hid[s, :, F:] = finish(both[:, :rem], both[:, MW // 2:MW // 2 + rem], tail)

    with scope("gate_value0"):
        gate_value(0)
    with scope("relay_dn_a"):
        for a in range(DN, DN + DN_PIECES):
            relay(a, 1)
    with scope("gate_value1"):
        gate_value(1)

    groups = [(i, g) for i in range(nz) for g in range(len(subs))]
    sc = {j: [tsem() for _ in range(2)] for j in groups}
    sx = {j: [[tsem() for _ in range(nx)] for _ in range(2)] for j in groups}
    zbase = tslot[0]
    tslot[0] += nz * ny
    turns = (1 - q, q)
    split = len(subs) > 1

    def down(j):
        i, g = j
        zz = zsrc(i)
        for k, s in enumerate(turns):
            for n, e in enumerate(subs[g]):
                yy = lax.rem(y + e, ny) if split else e
                part = jnp.dot(hid[s], dnb[zz, yy], preferred_element_type=F32).astype(BF16)
                for b in range(nx * 2):
                    pb[b % 2, i, g, s, b // 2, :, n * cw:(n + 1) * cw] = part[b * R:(b + 1) * R]
            send(pb.at[1 - c, i, g, s], rb.at[i, g, s], *sc[j][k], cpeer)

    def over_x(j):
        i, g = j
        for k, s in enumerate(turns):
            arrived(rb.at[i, g, s], *sc[j][k], cpeer)
            for b in range(nx):
                ab[i, g, s, b] = (pb[c, i, g, s, b].astype(F32) + rb[i, g, s, b].astype(F32)).astype(BF16)
            for d in range(1, nx):
                send(ab.at[i, g, s, lax.rem(x + d, nx)], xr.at[i, g, d - 1, s], *sx[j][k][d], xpeer(d))

    def place(j):
        i, g = j
        return zsrc(i), (lax.rem(y + subs[g][0], ny) if split else 0)

    def over_z(j):
        i, g = j
        zz, gg = place(j)
        for k, s in enumerate(turns):
            for d in range(1, nx):
                arrived(xr.at[i, g, d - 1, s], *sx[j][k][d], xpeer(d))
            acc = ab[i, g, s, x].astype(F32)
            for d in range(1, nx):
                acc = acc + xr[i, g, d - 1, s].astype(F32)
            zb[zz, gg, s] = acc.astype(BF16)
            if k == 0:
                n = zz * ny + gg
                send(zb.at[zz, gg, s], zr.at[zz, gg], ts.at[zbase + n], trs.at[zbase + n], ppeer)

    crossed, summed_up = [], []
    early = len(pending)

    def drain(n):
        for copy, cond in pending[:n]:
            when(cond, lambda copy=copy: copy.wait_send())
        del pending[:n]


    def flush(keep_x, keep_z):
        while len(crossed) > keep_x:
            j = crossed.pop(0)
            over_x(j)
            summed_up.append(j)
        while len(summed_up) > keep_z:
            over_z(summed_up.pop(0))

    for i in range(nz):
        for g in range(len(subs)):
            if (i, g) == (nz - 1, 0):
                with scope("drain"):
                    drain(early)
            with scope(f"complete_dn{i}{g}"):
                for e in subs[g]:
                    if not split and e == 0:
                        for b in range(1, ny):
                            for a in range(DN, DN + DN_PIECES):
                                complete(a, i, b)
                    if split and e > 0:
                        for a in range(DN, DN + DN_PIECES):
                            complete(a, i, ny - e)
            with scope(f"down{i}{g}"):
                down((i, g))
            crossed.append((i, g))
            flush(1, 2)
        if 0 < i + 1 < nz and i >= 1:
            pass
        if i + 2 < nz:
            with scope(f"relay_dn{i + 2}"):
                for a in range(DN, DN + DN_PIECES):
                    relay(a, i + 2)
    with scope("tail_x"):
        flush(0, 0)
    with scope("tail_z"):
        for zz in range(nz):
            for gg in range(len(subs)):
                n = zz * ny + gg
                arrived(zr.at[zz, gg], ts.at[zbase + n], trs.at[zbase + n], ppeer)
    with scope("final"):
        ffn_out = jnp.concatenate(
            [zb[zz, gg, q].astype(F32) + zr[zz, gg].astype(F32) for zz in range(nz) for gg in range(len(subs))],
            axis=1,
        )
        out[...] = (
            normalize(RESIDUAL_SCALE * mid[...].astype(F32) + ffn_out) * ogain[...].astype(F32)
        ).astype(BF16)
    with scope("drain_end"):
        drain(len(pending))


def shards(nf, nt, ny, tokens, gate_proj, signal_proj, spatial, signal_gain, mixer_out, mixer_gain, ffn_gate, ffn_value, conv_taps, ffn_down, output_gain):
    nz = nf // ny
    nx = nt // 2
    R, D = tokens.shape
    K, C = gate_proj.shape
    H = ffn_gate.shape[1]
    full = H // (2 * LANES) * LANES
    rem = H // 2 - full
    W = full + rem
    MW = -(-2 * rem // LANES) * LANES
    cw = mixer_out.shape[1]
    seq = nx * 2 * R
    subs = [(e,) for e in range(ny)] if cw % LANES == 0 else [tuple(range(ny))]
    gw = cw * len(subs[0])
    ns = len(subs)
    packed = bool(C % LANES or (2 * rem) % LANES)
    if packed:
        gp = jnp.concatenate([gate_proj, signal_proj], axis=1)
        gt, vt = ffn_gate[:, 2 * full:], ffn_value[:, 2 * full:]
    else:
        gp, gt, vt = gate_proj, ffn_gate, ffn_value

    vm = pltpu.VMEM
    n_w = GV_PIECES + DN_PIECES
    dma = pltpu.SemaphoreType.DMA
    n_t = 2 * nx + 2 * nx + 1 + nx + 1 + 4 * nx + nz * ns * (2 + 2 * nx) + nz * ny
    scratch = [
        vm((nz, ny, K, 2 * C), BF16),
        vm((nz, ny) + mixer_out.shape, BF16),
        vm((nz, ny, K, 2 * full + MW), BF16),
        vm((nz, ny, W, cw), BF16),
        vm((2, K, 2 * rem), BF16),
        vm((2, K, MW), BF16),
        vm((nx, 2, R, D), BF16),
        vm((2 * nx, 8, seq), F32),
        vm((2, nx, R, D), BF16),
        vm((nx, R, D), BF16),
        vm((nx, R, D), BF16),
        vm((nx - 1, R, D), BF16),
        vm((R, D), BF16),
        vm((2, nx, 2, R, D), BF16),
        vm((2, seq, W), BF16),
        vm((2, nz, ns, 2, nx, R, gw), BF16),
        vm((nz, ns, 2, nx, R, gw), BF16),
        vm((nz, ns, 2, nx, R, gw), BF16),
        vm((nz, ns, nx - 1, 2, R, gw), BF16),
        vm((nz, ns, 2, R, gw), BF16),
        vm((nz, ns, R, gw), BF16),
        dma((32,)),
        dma((nz,)),
        dma((nz,)),
        dma((nz, ny)),
        dma((nz, ny)),
        dma((nz,)),
        dma((nz,)),
        dma((nz, ny)),
        dma((nz, ny)),
        dma((n_w, nz)),
        dma((n_w, nz)),
        dma((n_w, nz, ny)),
        dma((n_w, nz, ny)),
        dma((n_t,)),
        dma((n_t,)),
    ]
    here, there = pl.BlockSpec(memory_space=pltpu.VMEM), pl.BlockSpec(memory_space=pl.ANY)
    return pl.pallas_call(
        functools.partial(kernel, nz, ny, nx, full, rem, subs, packed),
        out_shape=jax.ShapeDtypeStruct((R, D), BF16),
        in_specs=[here] + [there] * 8 + [here] * 5,
        out_specs=here,
        scratch_shapes=scratch,
        compiler_params=pltpu.CompilerParams(
            collective_id=0, has_side_effects=True, vmem_limit_bytes=67043328
        ),
    )(
        tokens, gp, signal_proj, mixer_out, ffn_gate, ffn_value, gt, vt, ffn_down, spatial,
        signal_gain[None], mixer_gain[None], conv_taps, output_gain[None],
    )


def solution(mesh):
    nf, nt = mesh.shape["fs"], mesh.shape["tp"]
    ny = 2 ** (int(math.log2(nf // 2)) // 2)
    in_specs = (
        P(("fs", "tp"), None),
        P("fs", "tp"),
        P("fs", "tp"),
        P(),
        P("tp"),
        P("tp", "fs"),
        P(),
        P("fs", "tp"),
        P("fs", "tp"),
        P(None, "tp"),
        P("tp", "fs"),
        P(),
    )
    return jax.shard_map(
        functools.partial(shards, nf, nt, ny),
        mesh=mesh,
        in_specs=in_specs,
        out_specs=P(("fs", "tp"), None),
        check_vma=False,
    )
```

time: 178 us -> 148 us (0.83)
  Pallas kernels: 169 us -> 144 us
  other arithmetic: 3.8 us -> 0 us
    pallas_call x1, Pallas kernels: 169 us -> 144 us  [shards(): pl.pallas_call(functools.partial(kernel, nz, ny, nx, full, rem, subs, pac...]
    another operation x5 -> x0, other arithmetic: 3.12 us -> none  [the longest x2 1.4 us: shards(): jnp.stack([jnp.concatenate([ffn_gate[:, :W], ffn_value[:, :W]], axis=1),...]
where the time goes in v1:
time: 148 us
  Pallas kernels  144 us (97%)
  local copies, waits for them, and re-layouts  3.79 us (3%)
    pallas_call x1, Pallas kernels, shards(): pl.pallas_call(functools.partial(kernel, nz, ny, nx, full, rem, subs, pac...  144 us

profile of v1, /device:TPU:0, one launch (start us, length us, event | category | flops | bytes accessed | tf_op | source)
XLA Modules:
  0.0 148.0 jit_solution(18069441524613419716)
XLA Ops:
  0.0 0.0 copy-start
  0.0 1.3 broadcast_in_dim.10.mgain
  1.3 0.0 copy-done
  1.3 0.6 broadcast_in_dim.11.ogain
  1.9 144.2 %shard_map.118 = bf16[128,2048]{1,0:T(8,128)(2,1)} custom-call(bf16[128,2048]{1,0:T(8,128)(2,1)} %tok.1, bf16[256,128]{1,0:T(8,128)(2,1)} %gp.1, bf16[256,128]{1,0:T(8,128)(2,1)} %sp_.1, bf16[128,256]{1,0:T(8,128)(2,1)} %mo.1, bf16[256,1408]{1,0:T(8,128)(2,1)} %gt.1, bf16[256,1408]{1,0:T(8,128)(2,1)} %vt.1, bf16[256,1408]{1,0:T(8,128)(2,1)} %gt.1, ...), custom_call_target="tpu_custom_call" | custom-call | tf_op jit(solution)/shard_map/pallas_call | solution.py:586
  146.1 1.9 %copy.14 = bf16[128,2048]{1,0:T(8,128)(2,1)} copy(bf16[128,2048]{1,0:T(8,128)(2,1)} %shard_map.118) | data formatting | bytes 1048576
Async XLA Ops:
  0.0 1.3 copy-start

commit v2 on v1

v2 whole, which is shorter than its diff:
```python
import functools
import math

import jax
import jax.numpy as jnp
from jax import lax
from jax.experimental import pallas as pl
from jax.experimental.pallas import tpu as pltpu
from jax.sharding import PartitionSpec as P

MIX_WIDTH = 512
HEAD_SIZE = 128
BLOCK = 128
SEGMENT = 64
LANES = 128
TILES = 5
DN_PIECES = 2
KEEP_X, KEEP_Z = 1, 4
EPSILON = 1e-05
RESIDUAL_SCALE = math.sqrt(2.0)
MESH = pl.DeviceIdType.MESH
F32 = jnp.float32
BF16 = jnp.bfloat16


def normalize(values):
    row_mean = jnp.mean(values, axis=-1, keepdims=True)
    centred = values - row_mean
    spread = jnp.mean(centred * centred, axis=-1, keepdims=True)
    return centred * lax.rsqrt(spread + EPSILON)


def wide(gain):
    return gain[...].astype(F32)[None]


def plan(*words):
    return tuple(
        (w[0], int(w[1], 16), d) for w in words for d in ((1, 2, 3) if w[2] == "*" else (int(w[2]),))
    )


PLAN_Y0 = plan("o00")
PLAN_Y = plan("o10", "o20", "o30", "o40", "o50")
PLAN_FIRST = plan()
PLAN_M0 = plan("m00", "m10", "m20")
PLAN_M = plan()
PLAN_0 = plan("i01", "i02", "w00", "i11", "i12", "w10", "i21", "i22", "w20")
PLAN_A = plan("r01", "r02", "r03", "r11", "n30")
PLAN_B = plan("i31", "n40", "i41", "n50", "i51", "r12", "r21", "r13", "r22", "r23")
PLAN_C = plan("e30", "r31", "o60", "o70")
PLAN_D = plan("e40", "r41", "e50", "i61", "n60", "r51", "r32", "r33", "i71", "e60", "r42", "r43", "n70", "e70", "r52", "r53")
PLAN_E = {0: plan("r61"), 2: plan("r71")}
PLAN_H = {(0, 0): plan("r62"), (0, 1): plan("r63"), (1, 0): plan("r72"), (1, 1): plan("r73")}


def kernel(
    nz, ny, nx, full, rem, subs, packed, dn_pieces,
    tok, gp, sp_, mo, fg, fv, gt, vt, dn, spatial, sgain, mgain, taps, ogain,
    out,
    gsb, mob, gvb, gtb, dnb, tails, mixed, xin, stat, pm, prc, abm, pxr, mid, hin, hid, pb, rb, ab, xr, zb, zr,
    loc_sem, gzr, mzr, gvr, gvy, dnr, shared, ts,
):
    R, D = tok.shape
    C, cw = mo.shape
    K = fg.shape[0]
    F = full
    W = full + rem
    MW = mixed.shape[2]
    f = lax.axis_index("fs")
    t = lax.axis_index("tp")
    z, y = f // ny, f % ny
    x, c = t // 2, t % 2
    q = z % 2
    seq = nx * 2 * R
    gw = ny * cw

    def zsrc(d):
        zz = z
        for bit in (1 << k for k in range(d.bit_length())):
            if d & bit:
                zz = zz + bit - 2 * bit * ((z // bit) % 2)
        return zz

    def zpeer(d):
        return (zsrc(d) * ny + y, t)

    inner = ((z + 1) // 2) % 2

    def source(k):
        if nz != 4 or k < 2:
            return k, zsrc(k)
        return (3 - inner, 3 - 3 * (z // 2)) if k == 2 else (2 + inner, 2 - z // 2)

    def ypeer(e):
        return (z * ny + lax.rem(y + e, ny), t)

    def xpeer(d):
        return (f, lax.rem(x + d, nx) * 2 + c)

    def tpeer(d, e):
        return (f, lax.rem(x + d, nx) * 2 + (c if e == 0 else 1 - c))

    cpeer = (f, x * 2 + 1 - c)
    ppeer = ((z + 1 - 2 * q) * ny + y, t)

    def ysrc(e):
        return lax.rem(y + ny - e, ny)

    def xsrc(d):
        return lax.rem(x + nx - d, nx)

    names = {}

    def common(name):
        return shared.at[names.setdefault(name, len(names))]

    def remote(src, dst, ssem, rsem, to):
        return pltpu.make_async_remote_copy(
            src_ref=src, dst_ref=dst, send_sem=ssem, recv_sem=rsem, device_id=to, device_id_type=MESH
        )

    def send(kind, src, dst, rsem, to):
        remote(src, dst, common(kind), rsem, to).start()

    def arrived(dst, rsem):
        pltpu.make_async_copy(dst, dst, rsem).wait()

    def sent(kind, whole):
        pltpu.make_async_copy(whole, whole, common(kind)).wait()

    scope = jax.named_scope
    tslot = [0]

    def tsem():
        k = tslot[0]
        tslot[0] += 1
        return ts.at[k]

    dn_rows = W // dn_pieces
    tiles = F // LANES
    DN = tiles + 1

    def parts(a, h, zz, yy):
        if a < tiles:
            at = pl.ds(pl.multiple_of(h * F + a * LANES, LANES), LANES)
            dst = gvb.at[a, zz, yy]
            return [(fg.at[:, at], dst.at[:, pl.ds(0, LANES)]), (fv.at[:, at], dst.at[:, pl.ds(LANES, LANES)])]
        if a < DN:
            return [(mixed.at[h], gtb.at[zz, yy])]
        lo, hi = (a - DN) * dn_rows, (a - DN + 1) * dn_rows
        dst = dnb.at[zz, yy]
        found = []
        if lo < F:
            n = min(hi, F) - lo
            found.append((dn.at[pl.ds(pl.multiple_of(h * F + lo, 16), n)], dst.at[pl.ds(lo, n)]))
        if hi > F:
            s = max(lo, F)
            n = hi - s
            found.append(
                (dn.at[pl.ds(pl.multiple_of(2 * F + h * rem + s - F, 16), n)], dst.at[pl.ds(s, n)])
            )
        return found

    def slot(a, zz, yy):
        if a < tiles:
            return gvb.at[a, zz, yy]
        if a < DN:
            return gtb.at[zz, yy]
        return dnb.at[zz, yy, pl.ds((a - DN) * dn_rows, dn_rows)]

    def fetch(k, src, dst):
        pltpu.make_async_copy(src, dst, loc_sem.at[k]).start()

    def ready(k, whole):
        pltpu.make_async_copy(whole, whole, loc_sem.at[k]).wait()

    GS, MO, TAILS, GV, DOWN = range(5)
    if packed:
        fetch(GS, gp, gsb.at[z, y])
    else:
        fetch(GS, gp, gsb.at[z, y, :, pl.ds(0, C)])
        fetch(GS, sp_, gsb.at[z, y, :, pl.ds(C, C)])
    fetch(MO, mo, mob.at[z, y])
    T = tails.shape[2]
    if packed:
        fetch(TAILS, gt, tails.at[0])
        fetch(TAILS, vt, tails.at[1])
    else:
        fetch(TAILS, gt.at[:, pl.ds(2 * F, T)], tails.at[0])
        fetch(TAILS, vt.at[:, pl.ds(2 * F, T)], tails.at[1])
    for a in range(tiles):
        for src, dst in parts(a, q, z, y):
            fetch(GV, src, dst)
    for a in range(DN, DN + dn_pieces):
        for src, dst in parts(a, q, z, y):
            fetch(DOWN, src, dst)

    barrier = pltpu.get_barrier_semaphore()
    peers = [zpeer(d) for d in range(1, nz)] + [ypeer(e) for e in range(1, ny)]
    peers += [tpeer(d, e) for d in range(nx) for e in range(2) if d + e]
    for p in peers:
        pl.semaphore_signal(barrier, inc=1, device_id=p, device_id_type=MESH)

    ready(TAILS, tails)
    for h in range(2):
        for k in range(2):
            mixed[h, :, k * (MW // 2):k * (MW // 2) + rem] = tails[k, :, h * rem:(h + 1) * rem]
    for k in range(2):
        part = tails[k].astype(F32)
        part = jnp.where(q == 0, part[:, :rem], part[:, rem:2 * rem]).astype(BF16)
        gtb[z, y, :, k * (MW // 2):k * (MW // 2) + rem] = part
    ready(GS, gsb.at[z, y])
    ready(MO, mob.at[z, y])
    pl.semaphore_wait(barrier, len(peers))

    def issue_z(a, d):
        for src, dst in parts(a, zsrc(d) % 2, z, y):
            remote(src, dst, common(family(a) + "_z"), z_sem(a, d), zpeer(d)).start()

    def z_sem(a, d):
        return gvr.at[a, d] if a < DN else dnr.at[a - DN, d]

    def y_sem(a, d, e):
        return gvy.at[a, e] if a < DN else dnr.at[dn_pieces + e - 1, d]

    def family(a):
        return "gv" if a < tiles else "gt" if a < DN else "dn"

    def issue_y(a):
        for e in range(1, ny):
            send(family(a) + "_y", slot(a, z, y), slot(a, z, y), y_sem(a, 0, e), ypeer(e))

    def relay(a, k):
        d, zz = source(k)
        arrived(slot(a, zz, y), z_sem(a, d))
        for e in range(1, ny):
            send(family(a) + "_y", slot(a, zz, y), slot(a, zz, y), y_sem(a, d, e), ypeer(e))

    bits = [1 << k for k in reversed(range((nz - 1).bit_length()))]

    def spread(kind, buf, d, rsem):
        src = zsrc(d)
        for bit in bits:
            if d == 0 or bit < (d & -d):
                send(kind, buf(src), buf(src), rsem.at[d | bit], zpeer(bit))

    def issue_far(a, what):
        if nz != 4:
            for d in range(2, nz):
                if (what == "n") == (d == 2) and what != "w" and (what != "m" or d > 2):
                    issue_z(a, d)
            return
        if what in "mw":
            pl.when(inner == (1 if what == "m" else 0))(lambda: issue_z(a, 3))
            return
        row = 2 - z // 2 if what == "n" else 3 - 3 * (z // 2)
        d = 2 + inner if what == "n" else 3 - inner
        for src, dst in parts(a, row % 2, z, y):
            remote(src, dst, common(family(a) + "_z"), z_sem(a, d), (row * ny + y, t)).start()

    def steps(plan):
        for what, piece, d in plan:
            if piece < TILES and piece >= tiles:
                continue
            a = piece if piece < TILES else piece - TILES + tiles
            if what == "o":
                issue_y(a)
            elif what in "nemw":
                issue_far(a, what)
            for dd in range(1, nz):
                if dd == d or (d == 3 and dd > 3):
                    (relay if what == "r" else issue_z)(a, dd)

    def gs_block(src):
        return gsb.at[src, y]

    def mo_block(src):
        return mob.at[src]

    spread("gs_z", gs_block, 0, gzr)
    for e in range(1, ny):
        send("mo_y", mob.at[z, y], mob.at[z, y], common(f"mo_y{e}r"), ypeer(e))
    for e in range(1, ny):
        send("gs_y", gsb.at[z, y], gsb.at[z, y], common(f"gs_y{e}r"), ypeer(e))
    ready(GV, gvb.at[:, z, y])
    steps(PLAN_Y0)
    steps(PLAN_FIRST)

    xin[x, c] = normalize(tok[...].astype(F32)).astype(BF16)
    s1 = [tsem() for _ in range(nx)]
    for d in range(1, nx):
        send("xin_x", xin.at[x, c], xin.at[x, c], s1[d], xpeer(d))
    send("xin_c", xin.at[x, c], xin.at[x, c], common("xin_cr"), cpeer)

    with scope("mo_y"):
        for e in range(1, ny):
            arrived(mob.at[z, ysrc(e)], common(f"mo_y{e}r"))
    spread("mo_z", mo_block, 0, mzr)
    steps(PLAN_M0)
    for d in range(1, nz):
        with scope(f"relay_gs{d}"):
            arrived(gs_block(zsrc(d)), gzr.at[d])
            spread("gs_z", gs_block, d, gzr)
            for e in range(1, ny):
                send("gs_y", gs_block(zsrc(d)), gs_block(zsrc(d)), common(f"gs_y{e}r"), ypeer(e))
    steps(PLAN_M)
    for d in range(1, nz):
        with scope(f"relay_mo{d}"):
            arrived(mo_block(zsrc(d)), mzr.at[d])
            spread("mo_z", mo_block, d, mzr)
    with scope("first_z"):
        steps(PLAN_0)
    ready(DOWN, dnb.at[z, y])
    steps(PLAN_Y)
    with scope("xin"):
        for d in range(1, nx):
            arrived(xin.at[xsrc(d), c], s1[d])
            send("xin_c", xin.at[xsrc(d), c], xin.at[xsrc(d), c], common("xin_cr"), cpeer)
        arrived(xin.at[:, 1 - c], common("xin_cr"))
    with scope("complete_gs"):
        for e in range(1, ny):
            arrived(gsb.at[:, ysrc(e)], common(f"gs_y{e}r"))

    with scope("mix_in"):
        pre = jnp.dot(xin[...].reshape(seq, D), gsb[...].reshape(D, 2 * C), preferred_element_type=F32)
        branch_signal = jax.nn.gelu(pre[:, C:])
        total = jnp.sum(branch_signal, axis=1, keepdims=True)
        square = jnp.sum(branch_signal * branch_signal, axis=1, keepdims=True)
        lane = lax.broadcasted_iota(jnp.int32, (seq, LANES), 1)
        stat[0] = jnp.where(lane == 0, total, square).T[:8]
    others = [(d, e) for d in range(nx) for e in range(2) if d + e]
    sx = {}
    for d, e in others:
        sx[d, e] = tsem()
        send("stat", stat.at[0], stat.at[2 * d + e], sx[d, e], tpeer(d, e))
    branch_gate = jax.nn.gelu(pre[:, :C])
    with scope("stats"):
        summed = stat[0]
        for d, e in others:
            arrived(stat.at[2 * d + e], sx[d, e])
            summed = summed + stat[2 * d + e]
    with scope("mix_out"):
        back = summed.T
        row_mean = back[:, 0:1] / MIX_WIDTH
        spread = back[:, 1:2] / MIX_WIDTH - row_mean * row_mean
        spatial_input = (
            (branch_signal - row_mean) * lax.rsqrt(spread + EPSILON) * wide(sgain)
        ).astype(BF16)
        rows_i = lax.broadcasted_iota(jnp.int32, (BLOCK, BLOCK), 0) // SEGMENT
        cols_i = lax.broadcasted_iota(jnp.int32, (BLOCK, BLOCK), 1) // SEGMENT
        own = spatial[t * C // HEAD_SIZE]
        own = jnp.where(cols_i <= rows_i, own, jnp.zeros_like(own))
        gated = jnp.concatenate(
            [
                branch_gate[b * BLOCK:(b + 1) * BLOCK]
                * jnp.dot(own, spatial_input[b * BLOCK:(b + 1) * BLOCK], preferred_element_type=F32)
                for b in range(seq // BLOCK)
            ],
            axis=0,
        ).astype(BF16)
        for k in range(nz * ny):
            part = jnp.dot(gated, mob[k // ny, k % ny], preferred_element_type=F32).astype(BF16)
            for b in range(nx * 2):
                pm[b % 2, b // 2, :, k * cw:(k + 1) * cw] = part[b * R:(b + 1) * R]
    sc = tsem()
    send("pm", pm.at[1 - c], prc, sc, cpeer)
    with scope("mix_core"):
        arrived(prc, sc)
    for b in range(nx):
        abm[b] = (pm[c, b].astype(F32) + prc[b].astype(F32)).astype(BF16)
    sx = [tsem() for _ in range(nx)]
    for d in range(1, nx):
        send("abm", abm.at[lax.rem(x + d, nx)], pxr.at[d - 1], sx[d], xpeer(d))
    with scope("relay_gv0"):
        steps(PLAN_A)
    with scope("mix_x"):
        for d in range(1, nx):
            arrived(pxr.at[d - 1], sx[d])
    with scope("mid"):
        mix_out = pm[c, x].astype(F32) + prc[x].astype(F32)
        for d in range(1, nx):
            mix_out = mix_out + pxr[d - 1].astype(F32)
        mid[...] = (
            normalize(RESIDUAL_SCALE * tok[...].astype(F32) + mix_out) * wide(mgain)
        ).astype(BF16)
        hin[q, x, c] = normalize(mid[...].astype(F32)).astype(BF16)

    sp = tsem()
    send("hin_z", hin.at[q, x, c], hin.at[q, x, c], sp, ppeer)
    sx = [[tsem() for _ in range(nx)] for _ in range(2)]

    def rows_out(k, s):
        for d in range(1, nx):
            send("hin_x", hin.at[s, x, c], hin.at[s, x, c], sx[k][d], xpeer(d))
        send("hin_c", hin.at[s, x, c], hin.at[s, x, c], common("hin_cr"), cpeer)

    def rows_over(k, s):
        for d in range(1, nx):
            arrived(hin.at[s, xsrc(d), c], sx[k][d])
            send("hin_c", hin.at[s, xsrc(d), c], hin.at[s, xsrc(d), c], common("hin_cr"), cpeer)

    rows_out(0, q)
    with scope("relay_b"):
        steps(PLAN_B)
    with scope("rows_x0"):
        rows_over(0, q)
    with scope("relay_c"):
        steps(PLAN_C)
    with scope("pair_rows"):
        arrived(hin.at[1 - q, x, c], sp)
    rows_out(1, 1 - q)
    with scope("relay_d"):
        steps(PLAN_D)
    with scope("rows_x1"):
        rows_over(1, 1 - q)
    with scope("rows_core"):
        arrived(hin.at[:, :, 1 - c], common("hin_cr"))
    def gate_value(a):
        lhs_rows = (hin[s].reshape(seq, D) for s in range(2))
        if a < tiles:
            weights = gvb[a].reshape(D, 2 * LANES)
            tap = taps[:, pl.ds(pl.multiple_of(q * F + a * LANES, LANES), LANES)].astype(F32)
            n, at = LANES, LANES
        else:
            weights = gtb[...].reshape(D, MW)
            tap = taps[:, 2 * F:2 * F + 2 * rem].astype(F32)
            tap = jnp.where(q == 0, tap[:, :rem], tap[:, rem:])
            n, at = rem, MW // 2
        for s, lhs in enumerate(lhs_rows):
            both = jnp.dot(lhs, weights, preferred_element_type=F32)
            gate, value = both[:, :n], both[:, at:at + n]
            row = lax.broadcasted_iota(jnp.int32, gate.shape, 0)
            one = jnp.where(row >= 1, pltpu.roll(gate, 1, 0), 0.0)
            two = jnp.where(row >= 2, pltpu.roll(gate, 2, 0), 0.0)
            conv = tap[0:1] * two + tap[1:2] * one + tap[2:3] * gate
            hid[s, :, a * LANES:a * LANES + n] = (jax.nn.silu(conv) * value).astype(BF16)

    for a in range(DN):
        with scope(f"complete_gv{a}"):
            for e in range(1, ny):
                whole = gvb.at[a, :, ysrc(e)] if a < tiles else gtb.at[:, ysrc(e)]
                arrived(whole, gvy.at[a, e])
        with scope(f"gate_value{a}"):
            gate_value(a)
        with scope("relay_e"):
            steps(PLAN_E.get(a if a < tiles else TILES, ()))

    groups = sorted(
        ((i, g) for i in range(nz) for g in range(len(subs))),
        key=lambda j: (j[0] >= nz // 2, j[1] > 0 and j[0] >= nz // 2, j),
    )
    sc = {j: [tsem() for _ in range(2)] for j in groups}
    sx = {j: [[tsem() for _ in range(nx)] for _ in range(2)] for j in groups}
    turns = (1 - q, q)
    split = len(subs) > 1

    def down(item):
        (i, g), k = item
        s, zz = turns[k], source(i)[1]
        for n, e in enumerate(subs[g]):
            yy = lax.rem(y + e, ny) if split else e
            part = jnp.dot(hid[s], dnb[zz, yy], preferred_element_type=F32).astype(BF16)
            for b in range(nx * 2):
                pb[b % 2, i, g, s, b // 2, :, n * cw:(n + 1) * cw] = part[b * R:(b + 1) * R]
        send("pb", pb.at[1 - c, i, g, s], rb.at[i, g, s], sc[i, g][k], cpeer)
        crossed.append(item)

    def over_x(item):
        (i, g), k = item
        s = turns[k]
        arrived(rb.at[i, g, s], sc[i, g][k])
        for b in range(nx):
            ab[i, g, s, b] = (pb[c, i, g, s, b].astype(F32) + rb[i, g, s, b].astype(F32)).astype(BF16)
        for d in range(1, nx):
            send("ab", ab.at[i, g, s, lax.rem(x + d, nx)], xr.at[i, g, d - 1, s], sx[i, g][k][d], xpeer(d))

    def over_z(item):
        (i, g), k = item
        s, zz = turns[k], source(i)[1]
        gg = lax.rem(y + subs[g][0], ny) if split else 0
        for d in range(1, nx):
            arrived(xr.at[i, g, d - 1, s], sx[i, g][k][d])
        acc = ab[i, g, s, x].astype(F32)
        for d in range(1, nx):
            acc = acc + xr[i, g, d - 1, s].astype(F32)
        zb[zz, gg, s] = acc.astype(BF16)
        if k == 0:
            send("zb", zb.at[zz, gg, s], zr.at[zz, gg], common("zbr"), ppeer)

    crossed, summed_up = [], []
    def flush(keep_x, keep_z):
        while len(crossed) > keep_x:
            j = crossed.pop(0)
            over_x(j)
            summed_up.append(j)
        while len(summed_up) > keep_z:
            over_z(summed_up.pop(0))

    def complete_dn(j):
        i, g = j
        with scope(f"complete_dn{i}{g}"):
            for e in range(1, ny):
                if (split and e in subs[g]) or not split:
                    b = ny - e if split else e
                    d, zz = source(i)
                    arrived(dnb.at[zz, ysrc(b)], dnr.at[dn_pieces + b - 1, d])

    for j in groups:
        complete_dn(j)
        with scope(f"down{j[0]}{j[1]}"):
            down((j, 0))
            down((j, 1))
        with scope(f"relay_h{j[0]}"):
            steps(PLAN_H.get(j, ()) if split else PLAN_H.get((j[0], 0), ()) + PLAN_H.get((j[0], 1), ()))
        with scope(f"flush{j[0]}{j[1]}"):
            flush(KEEP_X, KEEP_Z)
    with scope("tail_x"):
        flush(0, 0)
    with scope("tail_z"):
        arrived(zr, common("zbr"))
    with scope("final"):
        ffn_out = jnp.concatenate(
            [zb[zz, gg, q].astype(F32) + zr[zz, gg].astype(F32) for zz in range(nz) for gg in range(len(subs))],
            axis=1,
        )
        out[...] = (
            normalize(RESIDUAL_SCALE * mid[...].astype(F32) + ffn_out) * wide(ogain)
        ).astype(BF16)
    with scope("drain_end"):
        sent("gs_z", gsb.at[pl.ds(0, nz - 1), y])
        sent("mo_z", mob.at[pl.ds(0, nz - 1)])
        far = pl.ds(0, nz - 1)
        sent("gv_z", gvb.at[:, far, y])
        sent("gt_z", gtb.at[far, y])
        sent("dn_z", dnb.at[far, y])
        over_y = pl.ds(0, ny - 1)
        sent("mo_y", mob.at[z, over_y])
        sent("gs_y", gsb.at[:, over_y])
        sent("gv_y", gvb.at[:, :, over_y])
        sent("gt_y", gtb.at[:, over_y])
        sent("dn_y", dnb.at[:, over_y])
        sent("xin_x", xin.at[pl.ds(0, nx - 1), 0])
        sent("xin_c", xin.at[:, c])
        sent("stat", stat.at[pl.ds(0, 2 * nx - 1)])
        sent("pm", prc)
        sent("abm", pxr)
        sent("hin_z", hin.at[q, x, c])
        sent("hin_x", hin.at[:, pl.ds(0, nx - 1), c])
        sent("hin_c", hin.at[:, :, c])
        sent("pb", rb)
        sent("ab", xr)
        sent("zb", zr)


def shards(nf, nt, ny, tokens, gate_proj, signal_proj, spatial, signal_gain, mixer_out, mixer_gain, ffn_gate, ffn_value, conv_taps, ffn_down, output_gain):
    nz = nf // ny
    nx = nt // 2
    R, D = tokens.shape
    K, C = gate_proj.shape
    H = ffn_gate.shape[1]
    full = H // (2 * LANES) * LANES
    rem = H // 2 - full
    W = full + rem
    MW = -(-2 * rem // LANES) * LANES
    cw = mixer_out.shape[1]
    seq = nx * 2 * R
    subs = [(e,) for e in range(ny)] if cw % LANES == 0 else [tuple(range(ny))]
    gw = cw * len(subs[0])
    ns = len(subs)
    dn_pieces = DN_PIECES
    packed = bool(C % LANES or (2 * rem) % LANES)
    if packed:
        gp = jnp.concatenate([gate_proj, signal_proj], axis=1)
        gt, vt = ffn_gate[:, 2 * full:], ffn_value[:, 2 * full:]
    else:
        gp, gt, vt = gate_proj, ffn_gate, ffn_value

    vm = pltpu.VMEM
    dma = pltpu.SemaphoreType.DMA
    n_t = 6 * nx + 2 + nz * ns * (2 + 2 * nx)
    scratch = [
        vm((nz, ny, K, 2 * C), BF16),
        vm((nz, ny) + mixer_out.shape, BF16),
        vm((full // LANES, nz, ny, K, 2 * LANES), BF16),
        vm((nz, ny, K, MW), BF16),
        vm((nz, ny, W, cw), BF16),
        vm((2, K, 2 * rem), BF16),
        vm((2, K, MW), BF16),
        vm((nx, 2, R, D), BF16),
        vm((2 * nx, 8, seq), F32),
        vm((2, nx, R, D), BF16),
        vm((nx, R, D), BF16),
        vm((nx, R, D), BF16),
        vm((nx - 1, R, D), BF16),
        vm((R, D), BF16),
        vm((2, nx, 2, R, D), BF16),
        vm((2, seq, W), BF16),
        vm((2, nz, ns, 2, nx, R, gw), BF16),
        vm((nz, ns, 2, nx, R, gw), BF16),
        vm((nz, ns, 2, nx, R, gw), BF16),
        vm((nz, ns, nx - 1, 2, R, gw), BF16),
        vm((nz, ns, 2, R, gw), BF16),
        vm((nz, ns, R, gw), BF16),
        dma((5,)),
        dma((nz,)),
        dma((nz,)),
        dma((full // LANES + 1, nz)),
        dma((full // LANES + 1, ny)),
        dma((dn_pieces + ny - 1, nz)),
        dma((24 + 2 * (ny - 1),)),
        dma((n_t,)),
    ]
    here, there = pl.BlockSpec(memory_space=pltpu.VMEM), pl.BlockSpec(memory_space=pl.ANY)
    return pl.pallas_call(
        functools.partial(kernel, nz, ny, nx, full, rem, subs, packed, dn_pieces),
        out_shape=jax.ShapeDtypeStruct((R, D), BF16),
        in_specs=[here] + [there] * 8 + [here] * 5,
        out_specs=here,
        scratch_shapes=scratch,
        compiler_params=pltpu.CompilerParams(
            collective_id=0, has_side_effects=True, vmem_limit_bytes=67043328
        ),
    )(
        tokens, gp, signal_proj, mixer_out, ffn_gate, ffn_value, gt, vt, ffn_down, spatial,
        signal_gain, mixer_gain, conv_taps, output_gain,
    )


def solution(mesh):
    nf, nt = mesh.shape["fs"], mesh.shape["tp"]
    ny = 2 ** (int(math.log2(nf // 2)) // 2)
    in_specs = (
        P(("fs", "tp"), None),
        P("fs", "tp"),
        P("fs", "tp"),
        P(),
        P("tp"),
        P("tp", "fs"),
        P(),
        P("fs", "tp"),
        P("fs", "tp"),
        P(None, "tp"),
        P("tp", "fs"),
        P(),
    )
    return jax.shard_map(
        functools.partial(shards, nf, nt, ny),
        mesh=mesh,
        in_specs=in_specs,
        out_specs=P(("fs", "tp"), None),
        check_vma=False,
    )
```

time: 148 us -> 140 us (0.946)
  Pallas kernels: 144 us -> 138 us
  local copies, waits for them, and re-layouts: 3.79 us -> 1.88 us
    pallas_call x1, Pallas kernels: 144 us -> 138 us  [shards(): pl.pallas_call(functools.partial(kernel, nz, ny, nx, full, rem, subs, pac...]
    broadcast_in_dim x2 -> x0, local copies, waits for them, and re-layouts: 1.9 us -> none  [the longest x1 1.3 us: shards(): mixer_gain[None]]
where the time goes in v2:
time: 140 us; the launch traced here: 139 us
  Pallas kernels  138 us (99%)
  local copies, waits for them, and re-layouts  1.88 us (1%)
    pallas_call x1, Pallas kernels, shards(): pl.pallas_call(functools.partial(kernel, nz, ny, nx, full, rem, subs, pac...  138 us

profile of v2, /device:TPU:0, one launch (start us, length us, event | category | flops | bytes accessed | tf_op | source)
XLA Modules:
  0.0 139.4 jit_solution(5262241916081980780)
XLA Ops:
  0.0 137.5 %shard_map.118 = bf16[128,2048]{1,0:T(8,128)(2,1)} custom-call(bf16[128,2048]{1,0:T(8,128)(2,1)} %tok.1, bf16[256,128]{1,0:T(8,128)(2,1)} %gp.1, bf16[256,128]{1,0:T(8,128)(2,1)} %sp_.1, bf16[128,256]{1,0:T(8,128)(2,1)} %mo.1, bf16[256,1408]{1,0:T(8,128)(2,1)} %gt.1, bf16[256,1408]{1,0:T(8,128)(2,1)} %vt.1, bf16[256,1408]{1,0:T(8,128)(2,1)} %gt.1, ...), custom_call_target="tpu_custom_call" | custom-call | tf_op jit(solution)/shard_map/pallas_call | solution.py:615
  137.5 1.9 %copy.14 = bf16[128,2048]{1,0:T(8,128)(2,1)} copy(bf16[128,2048]{1,0:T(8,128)(2,1)} %shard_map.118) | data formatting | bytes 1048576

commit v3 on v2

--- a/solution.py
+++ b/solution.py
@@ -15,7 +15,7 @@
 LANES = 128
 TILES = 5
 DN_PIECES = 2
-KEEP_X, KEEP_Z = 1, 4
+KEEP_X, KEEP_Z = 0, 4
 EPSILON = 1e-05
 RESIDUAL_SCALE = math.sqrt(2.0)
 MESH = pl.DeviceIdType.MESH
@@ -41,17 +41,17 @@
 
 
 PLAN_Y0 = plan("o00")
-PLAN_Y = plan("o10", "o20", "o30", "o40", "o50")
+PLAN_Y = plan("o10", "o20", "o30", "o40", "o50", "o60", "o70")
 PLAN_FIRST = plan()
 PLAN_M0 = plan("m00", "m10", "m20")
 PLAN_M = plan()
 PLAN_0 = plan("i01", "i02", "w00", "i11", "i12", "w10", "i21", "i22", "w20")
 PLAN_A = plan("r01", "r02", "r03", "r11", "n30")
 PLAN_B = plan("i31", "n40", "i41", "n50", "i51", "r12", "r21", "r13", "r22", "r23")
-PLAN_C = plan("e30", "r31", "o60", "o70")
-PLAN_D = plan("e40", "r41", "e50", "i61", "n60", "r51", "r32", "r33", "i71", "e60", "r42", "r43", "n70", "e70", "r52", "r53")
-PLAN_E = {0: plan("r61"), 2: plan("r71")}
-PLAN_H = {(0, 0): plan("r62"), (0, 1): plan("r63"), (1, 0): plan("r72"), (1, 1): plan("r73")}
+PLAN_C = plan("e30", "r31")
+PLAN_D = plan("e40", "r41", "e50", "n60", "r51", "i61", "r32", "e60", "r33", "i71", "n70", "r42", "r43", "e70", "r52", "r53")
+PLAN_E = {1: plan("r61"), 4: plan("r71")}
+PLAN_H = {(0, 0): plan("r62"), (0, 1): plan("r63"), (1, 0): plan(), (1, 1): plan("r72", "r73")}
 
 
 def kernel(

time: 140 us -> 137 us (0.979)
  Pallas kernels: 138 us -> 134 us
    pallas_call x1, Pallas kernels: 138 us -> 134 us  [shards(): pl.pallas_call(functools.partial(kernel, nz, ny, nx, full, rem, subs, pac...]
where the time goes in v3:
time: 137 us; the launch traced here: 136 us
  Pallas kernels  134 us (98%)
  local copies, waits for them, and re-layouts  1.88 us (1%)
    pallas_call x1, Pallas kernels, shards(): pl.pallas_call(functools.partial(kernel, nz, ny, nx, full, rem, subs, pac...  134 us

profile of v3, /device:TPU:0, one launch (start us, length us, event | category | flops | bytes accessed | tf_op | source)
XLA Modules:
  0.0 136.3 jit_solution(11374560607402738789)
XLA Ops:
  0.0 134.4 %shard_map.118 = bf16[128,2048]{1,0:T(8,128)(2,1)} custom-call(bf16[128,2048]{1,0:T(8,128)(2,1)} %tok.1, bf16[256,128]{1,0:T(8,128)(2,1)} %gp.1, bf16[256,128]{1,0:T(8,128)(2,1)} %sp_.1, bf16[128,256]{1,0:T(8,128)(2,1)} %mo.1, bf16[256,1408]{1,0:T(8,128)(2,1)} %gt.1, bf16[256,1408]{1,0:T(8,128)(2,1)} %vt.1, bf16[256,1408]{1,0:T(8,128)(2,1)} %gt.1, ...), custom_call_target="tpu_custom_call" | custom-call | tf_op jit(solution)/shard_map/pallas_call | solution.py:615
  134.5 1.9 %copy.14 = bf16[128,2048]{1,0:T(8,128)(2,1)} copy(bf16[128,2048]{1,0:T(8,128)(2,1)} %shard_map.118) | data formatting | bytes 1048576

commit v4 on v3

--- a/solution.py
+++ b/solution.py
@@ -45,7 +45,7 @@
 PLAN_FIRST = plan()
 PLAN_M0 = plan("m00", "m10", "m20")
 PLAN_M = plan()
-PLAN_0 = plan("i01", "i02", "w00", "i11", "i12", "w10", "i21", "i22", "w20")
+PLAN_0 = plan("i01", "i02", "w00", "i11", "i12", "w10", "i22", "w20", "i21")
 PLAN_A = plan("r01", "r02", "r03", "r11", "n30")
 PLAN_B = plan("i31", "n40", "i41", "n50", "i51", "r12", "r21", "r13", "r22", "r23")
 PLAN_C = plan("e30", "r31")

time: 137 us -> 136 us (level)
  no operation moved by 1% of the time
where the time goes in v4:
time: 136 us; the launch traced here: 135 us
  Pallas kernels  134 us (99%)
  local copies, waits for them, and re-layouts  1.88 us (1%)
    pallas_call x1, Pallas kernels, shards(): pl.pallas_call(functools.partial(kernel, nz, ny, nx, full, rem, subs, pac...  134 us

profile of v4, /device:TPU:0, one launch (start us, length us, event | category | flops | bytes accessed | tf_op | source)
XLA Modules:
  0.0 135.5 jit_solution(16827597690853898518)
XLA Ops:
  0.0 133.6 %shard_map.118 = bf16[128,2048]{1,0:T(8,128)(2,1)} custom-call(bf16[128,2048]{1,0:T(8,128)(2,1)} %tok.1, bf16[256,128]{1,0:T(8,128)(2,1)} %gp.1, bf16[256,128]{1,0:T(8,128)(2,1)} %sp_.1, bf16[128,256]{1,0:T(8,128)(2,1)} %mo.1, bf16[256,1408]{1,0:T(8,128)(2,1)} %gt.1, bf16[256,1408]{1,0:T(8,128)(2,1)} %vt.1, bf16[256,1408]{1,0:T(8,128)(2,1)} %gt.1, ...), custom_call_target="tpu_custom_call" | custom-call | tf_op jit(solution)/shard_map/pallas_call | solution.py:615
  133.6 1.9 %copy.14 = bf16[128,2048]{1,0:T(8,128)(2,1)} copy(bf16[128,2048]{1,0:T(8,128)(2,1)} %shard_map.118) | data formatting | bytes 1048576

commit v5 on v4

--- a/solution.py
+++ b/solution.py
@@ -40,8 +40,8 @@
     )
 
 
-PLAN_Y0 = plan("o00")
-PLAN_Y = plan("o10", "o20", "o30", "o40", "o50", "o60", "o70")
+PLAN_Y0 = plan("o00", "o50")
+PLAN_Y = plan("o10", "o20", "o30", "o40", "o60", "o70")
 PLAN_FIRST = plan()
 PLAN_M0 = plan("m00", "m10", "m20")
 PLAN_M = plan()

time: 136 us -> 136 us (level)
  no operation moved by 1% of the time
where the time goes in v5:
time: 136 us; the launch traced here: 135 us
  Pallas kernels  134 us (99%)
  local copies, waits for them, and re-layouts  1.88 us (1%)
    pallas_call x1, Pallas kernels, shards(): pl.pallas_call(functools.partial(kernel, nz, ny, nx, full, rem, subs, pac...  134 us

profile of v5, /device:TPU:0, one launch (start us, length us, event | category | flops | bytes accessed | tf_op | source)
XLA Modules:
  0.0 135.5 jit_solution(13128460254796524015)
XLA Ops:
  0.0 133.6 %shard_map.118 = bf16[128,2048]{1,0:T(8,128)(2,1)} custom-call(bf16[128,2048]{1,0:T(8,128)(2,1)} %tok.1, bf16[256,128]{1,0:T(8,128)(2,1)} %gp.1, bf16[256,128]{1,0:T(8,128)(2,1)} %sp_.1, bf16[128,256]{1,0:T(8,128)(2,1)} %mo.1, bf16[256,1408]{1,0:T(8,128)(2,1)} %gt.1, bf16[256,1408]{1,0:T(8,128)(2,1)} %vt.1, bf16[256,1408]{1,0:T(8,128)(2,1)} %gt.1, ...), custom_call_target="tpu_custom_call" | custom-call | tf_op jit(solution)/shard_map/pallas_call | solution.py:615
  133.6 1.9 %copy.14 = bf16[128,2048]{1,0:T(8,128)(2,1)} copy(bf16[128,2048]{1,0:T(8,128)(2,1)} %shard_map.118) | data formatting | bytes 1048576
